TPU v7x, 32 devices: a whole 2x2x4 slice. The times are simulated.
32 devices in a mesh: sp: 16 (over z, y, x), tp: 2 (over core).
Axes of the slice: x: 2, y: 2, z: 4, core: 2. Of those that a mesh axis runs over, the one named last changes fastest.
Arguments:
- resid: bfloat16 [4096, 2048], P('sp', 'tp'), may hold values from -6 to 6
- queries: bfloat16 [4096, 1024], P('sp', 'tp'), may hold values from -6 to 6
- keys_values: bfloat16 [8, 4096, 128], P('tp', 'sp'), may hold values from -6 to 6
- cum_gate: float32 [16, 4096], P('tp', 'sp'), as said below
- out_weight: bfloat16 [1024, 2048], P(None, 'tp'), may hold values from -1.5 to 1.5
- norm_gain: float32 [2048], replicated, may hold values from 0.1 to 1.9
- gate_weight: bfloat16 [2048, 5632], P('sp', 'tp'), may hold values from -0.125 to 0.125
- up_weight: bfloat16 [2048, 5632], P('sp', 'tp'), may hold values from -0.125 to 0.125
- conv_kernel: float32 [3, 2, 5632], P(None, None, 'tp'), may hold values from -3.5 to 3.5
- down_weight: bfloat16 [5632, 2048], P('tp', 'sp'), may hold values from -0.078125 to 0.078125
Outputs:
- layer_out: bfloat16 [4096, 2048], P('sp', 'tp')
Inputs may be any that keep to these rules, and one draw needn't show every extreme that they name: `cum_gate`: along positions each head's entries never increase.
All inputs are finite; a program needn't handle non-finite values.
Results may differ from a plain program's by a relative error of at most 0.015.
Values may be sent and summed in bfloat16 or wider, within the bound.
A program may use at most 128 MiB of HBM per device.

v0:
```python
import jax
import jax.numpy as jnp
from jax import lax
from jax.sharding import PartitionSpec as P

norm_eps = 1e-06


def from_behind(value, axis, by):
    size = lax.axis_size(axis)
    pairs = [(i, i + by) for i in range(size) if 0 <= i + by < size]
    return lax.ppermute(value, axis, pairs)


def attend(queries, keys_values, cum_gate, row_start):
    tok_rows = queries.shape[0]
    local_pairs = keys_values.shape[0]
    head_dim = keys_values.shape[2] // 2
    local_heads = cum_gate.shape[0]
    group_size = local_heads // local_pairs
    score_scale = head_dim ** (-0.5)
    query_heads = queries.reshape(tok_rows, local_pairs, group_size, head_dim)
    all_gates = lax.all_gather(cum_gate, "sp", axis=1, tiled=True)
    own_gates = lax.dynamic_slice_in_dim(all_gates, row_start, tok_rows, 1).reshape(
        local_pairs, group_size, tok_rows
    )
    query_pos = row_start + jnp.arange(tok_rows, dtype=jnp.int32)
    last_row = row_start + tok_rows - 1

    def add_block(state_now, key_block, offset):
        block_width = key_block.shape[1]
        key_part = key_block[:, :, :head_dim]
        values = key_block[:, :, head_dim:]
        key_gates = lax.dynamic_slice_in_dim(all_gates, offset, block_width, 1).reshape(
            local_pairs, group_size, block_width
        )
        scores = (
            jnp.einsum("tkgd,krd->kgtr", query_heads, key_part, preferred_element_type=jnp.float32)
            * score_scale
        )
        scores = scores + own_gates[:, :, :, None] - key_gates[:, :, None, :]
        visible = query_pos[:, None] >= (offset + jnp.arange(block_width, dtype=jnp.int32))[None, :]
        scores = jnp.where(visible, scores, -1e30)
        running_max, running_sum, weighted = state_now
        next_max = jnp.maximum(running_max, jnp.max(scores, axis=3))
        weights = jnp.where(visible, jnp.exp(scores - next_max[:, :, :, None]), 0.0)
        shrink = jnp.exp(running_max - next_max)
        running_sum = running_sum * shrink + jnp.sum(weights, axis=3)
        weighted = weighted * shrink[:, :, :, None] + jnp.einsum(
            "kgtr,krd->kgtd",
            weights.astype(jnp.bfloat16),
            values,
            preferred_element_type=jnp.float32,
        )
        return (next_max, running_sum, weighted)

    start_state = (
        jnp.full((local_pairs, group_size, tok_rows), -1e30, jnp.float32),
        jnp.zeros((local_pairs, group_size, tok_rows), jnp.float32),
        jnp.zeros((local_pairs, group_size, tok_rows, head_dim), jnp.float32),
    )
    arrived = lax.all_gather(keys_values, "sp", axis=1, tiled=True)
    arrived_rows = arrived.shape[1]
    block_rows = 512

    def fold_block(block_index, inner):
        block_start = block_index * block_rows
        key_block = lax.dynamic_slice_in_dim(arrived, block_index * block_rows, block_rows, 1)
        return lax.cond(
            block_start <= last_row,
            lambda current: add_block(current, key_block, block_start),
            lambda current: current,
            inner,
        )

    running_max, running_sum, weighted = lax.fori_loop(
        0, arrived_rows // block_rows, fold_block, start_state
    )
    result = (weighted / running_sum[:, :, :, None]).transpose(2, 0, 1, 3)
    return result.reshape(tok_rows, local_heads * head_dim).astype(jnp.bfloat16)


def local(
    resid,
    queries,
    keys_values,
    cum_gate,
    out_weight,
    norm_gain,
    gate_weight,
    up_weight,
    conv_kernel,
    down_weight,
):
    tok_rows = resid.shape[0]
    hidden_cols = gate_weight.shape[1]
    row_start = lax.axis_index("sp") * tok_rows
    attn = attend(queries, keys_values, cum_gate, row_start)
    branch = jnp.dot(
        lax.all_gather(attn, "tp", axis=1, tiled=True),
        out_weight,
        preferred_element_type=jnp.float32,
    )
    middle = (resid.astype(jnp.float32) + branch).astype(jnp.bfloat16)
    middle_f32 = middle.astype(jnp.float32)
    middle_full = lax.all_gather(middle, "tp", axis=1, tiled=True).astype(jnp.float32)
    inverse = lax.rsqrt(jnp.mean(middle_full * middle_full, axis=1, keepdims=True) + norm_eps)
    normed = (middle_full * inverse * norm_gain).astype(jnp.bfloat16)
    gate_sum = jnp.dot(
        normed,
        lax.all_gather(gate_weight, "sp", axis=0, tiled=True),
        preferred_element_type=jnp.float32,
    )
    up_sum = jnp.dot(
        normed,
        lax.all_gather(up_weight, "sp", axis=0, tiled=True),
        preferred_element_type=jnp.float32,
    )
    pre_gate = gate_sum.astype(jnp.bfloat16)
    pre_up = up_sum.astype(jnp.bfloat16)
    reach_back = conv_kernel.shape[0] - 1
    joined = jnp.concatenate([pre_gate, pre_up], axis=1)
    before = from_behind(joined[tok_rows - reach_back :], "sp", 1)
    padded = jnp.concatenate([before, joined], axis=0).astype(jnp.float32)
    kernel = conv_kernel.reshape(reach_back + 1, 2 * hidden_cols)
    mixed = jnp.zeros((tok_rows, 2 * hidden_cols), jnp.float32)
    for offset in range(reach_back + 1):
        mixed = mixed + kernel[offset][None, :] * padded[offset : offset + tok_rows]
    hidden = (jax.nn.silu(mixed[:, :hidden_cols]) * mixed[:, hidden_cols:]).astype(jnp.bfloat16)
    partials = jnp.dot(
        hidden,
        lax.all_gather(down_weight, "sp", axis=1, tiled=True),
        preferred_element_type=jnp.float32,
    )
    channel_out = lax.psum_scatter(
        partials.astype(jnp.bfloat16), "tp", scatter_dimension=1, tiled=True
    ).astype(jnp.float32)
    return (middle_f32 + channel_out).astype(jnp.bfloat16)


def solution(mesh):
    return jax.shard_map(
        local,
        mesh=mesh,
        in_specs=(
            P("sp", "tp"),
            P("sp", "tp"),
            P("tp", "sp", None),
            P("tp", "sp"),
            P(None, "tp"),
            P(),
            P("sp", "tp"),
            P("sp", "tp"),
            P(None, None, "tp"),
            P("tp", "sp"),
        ),
        out_specs=P("sp", "tp"),
        check_vma=False,
    )
```

profile of v0, /device:TPU:25, one launch (start us, length us, event | category | flops | bytes accessed | tf_op | source)
XLA Modules:
  0.0 684.5 jit_solution(4768735813569886703)
XLA Ops:
  10.4 26.6 %all_gather.22 = f32[8,4096]{1,0:T(8,128)S(1)} all-gather(f32[8,256]{1,0:T(8,128)} %param.17), channel_id=1, replica_groups=mesh['sp'=16,'tp'=2] {'sp'}, dimensions={1}, use_global_device_ids=true | all-gather | bytes 139264 | tf_op jit(solution)/shard_map/all_gather | solution.py:23
  36.9 58.6 %all-gather.6.cloned.1.call-done = bf16[4,4096,128]{1,2,0:T(8,128)(2,1)} async-done(((bf16[4,256,128]{1,2,0:T(8,128)(2,1)}), bf16[4,4096,128]{1,2,0:T(8,128)(2,1)}) %all-gather.6.cloned.1.call-update) | async-done | bytes 4194320 | tf_op jit(solution)/shard_map/all_gather | solution.py:62
  95.6 68.1 %while.18 = (s32[]{:T(128)}, f32[4,2,256]{2,1,0:T(2,128)S(1)}, f32[4,2,256]{2,1,0:T(2,128)S(1)}, f32[4,2,256,64]{2,3,1,0:T(8,128)S(1)}, s32[]{:T(128)}, /*index=...) while((s32[]{:T(128)}, f32[4,2,256]{2,1,0:T(2,128)S(1)}, ...), condition=%wide.region_5.6_spmd.clone, body=%wide.region_0.5_spmd.clone.sunk | while | flops 288756480 | bytes 32014712 | solution.py:76
  95.6 9.7 %conditional.3 = ((f32[4,2,256]{2,1,0:T(2,128)S(1)}, f32[4,2,256]{2,1,0:T(2,128)S(1)}, f32[4,2,256,64]{2,3,1,0:T(8,128)S(1)})) conditional(s32[]{:T(128)} %convert_element_type.103, (f32[4,2,256]{2,1,0:T(2,128)S(1)}, f32[4,2,256]{2,1,0:T(2,128)S(1)}, f32[4,2,256,64]{2,3,1,0:T(8,128)S(1)}) %tuple.53, (s32[]{:T(128)}, s32[]{:T(128)}, ...), branch_computations={%region_1.0_spmd, %region_2.4_spmd} | conditional | flops 288756480 | bytes 32013442 | solution.py:69
  101.9 3.4 fusion.10
  105.3 9.7 %conditional.3 = ((f32[4,2,256]{2,1,0:T(2,128)S(1)}, f32[4,2,256]{2,1,0:T(2,128)S(1)}, f32[4,2,256,64]{2,3,1,0:T(8,128)S(1)})) conditional(s32[]{:T(128)} %convert_element_type.103, (f32[4,2,256]{2,1,0:T(2,128)S(1)}, f32[4,2,256]{2,1,0:T(2,128)S(1)}, f32[4,2,256,64]{2,3,1,0:T(8,128)S(1)}) %tuple.53, (s32[]{:T(128)}, s32[]{:T(128)}, ...), branch_computations={%region_1.0_spmd, %region_2.4_spmd} | conditional | flops 288756480 | bytes 32013442 | solution.py:69
  105.6 2.5 fusion.6
  111.6 3.4 fusion.10
  115.1 9.7 %conditional.3 = ((f32[4,2,256]{2,1,0:T(2,128)S(1)}, f32[4,2,256]{2,1,0:T(2,128)S(1)}, f32[4,2,256,64]{2,3,1,0:T(8,128)S(1)})) conditional(s32[]{:T(128)} %convert_element_type.103, (f32[4,2,256]{2,1,0:T(2,128)S(1)}, f32[4,2,256]{2,1,0:T(2,128)S(1)}, f32[4,2,256,64]{2,3,1,0:T(8,128)S(1)}) %tuple.53, (s32[]{:T(128)}, s32[]{:T(128)}, ...), branch_computations={%region_1.0_spmd, %region_2.4_spmd} | conditional | flops 288756480 | bytes 32013442 | solution.py:69
  115.3 2.5 fusion.6
  121.3 3.4 fusion.10
  124.8 9.7 %conditional.3 = ((f32[4,2,256]{2,1,0:T(2,128)S(1)}, f32[4,2,256]{2,1,0:T(2,128)S(1)}, f32[4,2,256,64]{2,3,1,0:T(8,128)S(1)})) conditional(s32[]{:T(128)} %convert_element_type.103, (f32[4,2,256]{2,1,0:T(2,128)S(1)}, f32[4,2,256]{2,1,0:T(2,128)S(1)}, f32[4,2,256,64]{2,3,1,0:T(8,128)S(1)}) %tuple.53, (s32[]{:T(128)}, s32[]{:T(128)}, ...), branch_computations={%region_1.0_spmd, %region_2.4_spmd} | conditional | flops 288756480 | bytes 32013442 | solution.py:69
  125.0 2.5 fusion.6
  131.0 3.4 fusion.10
  134.5 9.7 %conditional.3 = ((f32[4,2,256]{2,1,0:T(2,128)S(1)}, f32[4,2,256]{2,1,0:T(2,128)S(1)}, f32[4,2,256,64]{2,3,1,0:T(8,128)S(1)})) conditional(s32[]{:T(128)} %convert_element_type.103, (f32[4,2,256]{2,1,0:T(2,128)S(1)}, f32[4,2,256]{2,1,0:T(2,128)S(1)}, f32[4,2,256,64]{2,3,1,0:T(8,128)S(1)}) %tuple.53, (s32[]{:T(128)}, s32[]{:T(128)}, ...), branch_computations={%region_1.0_spmd, %region_2.4_spmd} | conditional | flops 288756480 | bytes 32013442 | solution.py:69
  140.8 3.4 fusion.10
  144.2 9.7 %conditional.3 = ((f32[4,2,256]{2,1,0:T(2,128)S(1)}, f32[4,2,256]{2,1,0:T(2,128)S(1)}, f32[4,2,256,64]{2,3,1,0:T(8,128)S(1)})) conditional(s32[]{:T(128)} %convert_element_type.103, (f32[4,2,256]{2,1,0:T(2,128)S(1)}, f32[4,2,256]{2,1,0:T(2,128)S(1)}, f32[4,2,256,64]{2,3,1,0:T(8,128)S(1)}) %tuple.53, (s32[]{:T(128)}, s32[]{:T(128)}, ...), branch_computations={%region_1.0_spmd, %region_2.4_spmd} | conditional | flops 288756480 | bytes 32013442 | solution.py:69
  150.5 3.4 fusion.10
  154.0 9.7 %conditional.3 = ((f32[4,2,256]{2,1,0:T(2,128)S(1)}, f32[4,2,256]{2,1,0:T(2,128)S(1)}, f32[4,2,256,64]{2,3,1,0:T(8,128)S(1)})) conditional(s32[]{:T(128)} %convert_element_type.103, (f32[4,2,256]{2,1,0:T(2,128)S(1)}, f32[4,2,256]{2,1,0:T(2,128)S(1)}, f32[4,2,256,64]{2,3,1,0:T(8,128)S(1)}) %tuple.53, (s32[]{:T(128)}, s32[]{:T(128)}, ...), branch_computations={%region_1.0_spmd, %region_2.4_spmd} | conditional | flops 288756480 | bytes 32013442 | solution.py:69
  160.2 3.4 fusion.10
  163.8 3.0 all_gather.23
  170.2 17.8 %all-gather.8.cloned.1.call-done = bf16[256,2048]{1,0:T(8,128)(2,1)} async-done(((bf16[256,1024]{1,0:T(8,128)(2,1)}), bf16[256,2048]{1,0:T(8,128)(2,1)}) %all-gather.8.cloned.1.call-update) | async-done | bytes 1048592 | tf_op jit(solution)/shard_map/all_gather | solution.py:106
  189.6 141.3 %all-gather.10.cloned.1.call-done = bf16[2048,2816]{1,0:T(8,128)(2,1)} async-done(((bf16[128,2816]{1,0:T(8,128)(2,1)}), bf16[2048,2816]{1,0:T(8,128)(2,1)}) %all-gather.10.cloned.1.call-update) | async-done | bytes 11534352 | tf_op jit(solution)/shard_map/all_gather | solution.py:111
  330.9 7.8 %convolution_convert_fusion.1 = bf16[256,2816]{1,0:T(8,128)(2,1)S(1)} fusion(bf16[2048,2816]{1,0:T(8,128)(2,1)} %all-gather.10.cloned.1.call-done, bf16[256,2048]{1,0:T(8,128)(2,1)} %all-gather.8.cloned.1.call-done, f32[2048]{0:T(1024)S(1)} %copy-done.6, f32[256]{0:T(256)S(1)} %add_rsqrt_fusion), kind=kOutput, calls=%fused_computation.31 | convolution fusion | flops 2955608064 | bytes 14033920 | tf_op jit(solution)/shard_map/dot_general | solution.py:109
  338.7 134.4 %all-gather.12.cloned.1.call-done = bf16[2048,2816]{1,0:T(8,128)(2,1)} async-done(((bf16[128,2816]{1,0:T(8,128)(2,1)}), bf16[2048,2816]{1,0:T(8,128)(2,1)}) %all-gather.12.cloned.1.call-update) | async-done | bytes 11534352 | tf_op jit(solution)/shard_map/all_gather | solution.py:116
  473.1 7.8 %convolution_convert_fusion = bf16[256,2816]{1,0:T(8,128)(2,1)S(1)} fusion(bf16[2048,2816]{1,0:T(8,128)(2,1)} %all-gather.12.cloned.1.call-done, bf16[256,2048]{1,0:T(8,128)(2,1)} %all-gather.8.cloned.1.call-done, f32[2048]{0:T(1024)S(1)} %copy-done.6, f32[256]{0:T(256)S(1)} %add_rsqrt_fusion), kind=kOutput, calls=%fused_computation.30 | convolution fusion | flops 2955608064 | bytes 14033920 | tf_op jit(solution)/shard_map/dot_general | solution.py:114
  481.0 3.1 collective-permute-start
  484.2 3.2 collective-permute-done
  488.2 3.5 fusion.19
  491.6 164.3 %all-gather.14.cloned.1.call-done = bf16[2816,2048]{1,0:T(8,128)(2,1)} async-done(((bf16[2816,128]{1,0:T(8,128)(2,1)}), bf16[2816,2048]{1,0:T(8,128)(2,1)}) %all-gather.14.cloned.1.call-update) | async-done | bytes 11534352 | tf_op jit(solution)/shard_map/all_gather | solution.py:132
  655.9 10.4 %convolution_convert_fusion.2 = bf16[256,2048]{1,0:T(8,128)(2,1)} fusion(bf16[2816,2048]{1,0:T(8,128)(2,1)} %all-gather.14.cloned.1.call-done, f32[256,5632]{1,0:T(8,128)} %fusion.19), kind=kOutput, calls=%fused_computation.37 | convolution fusion | flops 2957639680 | bytes 18350080 | tf_op jit(solution)/shard_map/dot_general | solution.py:130
  666.3 9.3 %reduce-scatter.2.cloned.1.call-done = bf16[256,1024]{1,0:T(8,128)(2,1)} async-done(((bf16[256,2048]{1,0:T(8,128)(2,1)}), bf16[256,1024]{1,0:T(8,128)(2,1)}) %reduce-scatter.2.cloned.1.call-update) | async-done | bytes 524304 | tf_op jit(solution)/shard_map/reduce_scatter | solution.py:135
  (138 shorter events, 47.5 us)
Async XLA Ops:
  6.5 160.2 %copy-start = (bf16[1024,1024]{1,0:T(8,128)(2,1)S(1)}, bf16[1024,1024]{1,0:T(8,128)(2,1)}, u32[]{:S(2)}) copy-start(bf16[1024,1024]{1,0:T(8,128)(2,1)} %param.18) | copy-start | bytes 6291460
  6.5 89.0 %all-gather.6.cloned.1.call-start = ((), (), s32[]{:S(2)}) async-start(), calls=%async_computation.1 | async-start | bytes 4456448 | tf_op jit(solution)/shard_map/all_gather | solution.py:62
  8.5 179.5 %all-gather.8.cloned.1.call-start = ((), (), s32[]{:S(2)}) async-start(), calls=%async_computation.2 | async-start | bytes 1572864 | tf_op jit(solution)/shard_map/all_gather | solution.py:106
  95.6 71.2 %copy-start.4 = (bf16[256,1024]{1,0:T(8,128)(2,1)S(1)}, bf16[256,1024]{1,0:T(8,128)(2,1)}, u32[]{:S(2)}) copy-start(bf16[256,1024]{1,0:T(8,128)(2,1)} %param.14) | copy-start | bytes 1572868
  98.3 2.0 copy-start.2
  108.1 2.0 copy-start.2
  117.8 2.0 copy-start.2
  127.5 2.0 copy-start.2
  137.2 2.0 copy-start.2
  147.0 2.0 copy-start.2
  156.7 2.0 copy-start.2
  163.8 167.1 %copy-start.6 = (f32[2048]{0:T(1024)S(1)}, f32[2048]{0:T(1024)}, u32[]{:S(2)}) copy-start(f32[2048]{0:T(1024)} %param.19) | copy-start | bytes 24580
  168.3 162.6 %all-gather.10.cloned.1.call-start = ((), (), s32[]{:S(2)}) async-start(), calls=%async_computation.3 | async-start | bytes 12255232 | tf_op jit(solution)/shard_map/all_gather | solution.py:111
  169.0 304.1 %all-gather.12.cloned.1.call-start = ((), (), s32[]{:S(2)}) async-start(), calls=%async_computation.4 | async-start | bytes 12255232 | tf_op jit(solution)/shard_map/all_gather | solution.py:116
  169.6 486.3 %all-gather.14.cloned.1.call-start = ((), (), s32[]{:S(2)}) async-start(), calls=%async_computation.5 | async-start | bytes 12255232 | tf_op jit(solution)/shard_map/all_gather | solution.py:132
  170.2 505.4 %reduce-scatter.2.cloned.1.call-start = ((), (), s32[]{:S(2)}) async-start(), calls=%async_computation.6 | async-start | bytes 1572864 | tf_op jit(solution)/shard_map/reduce_scatter | solution.py:135
  338.7 145.4 %copy-start.5 = (f32[3,2,2816]{2,1,0:T(2,128)S(1)}, f32[3,2,2816]{2,1,0:T(2,128)}, u32[]{:S(2)}) copy-start(f32[3,2,2816]{2,1,0:T(2,128)} %param.22) | copy-start | bytes 202756
  481.0 6.3 collective-permute-start
  491.6 184.0 %copy-start.3 = (bf16[256,1024]{1,0:T(8,128)(2,1)S(1)}, bf16[256,1024]{1,0:T(8,128)(2,1)}, u32[]{:S(2)}) copy-start(bf16[256,1024]{1,0:T(8,128)(2,1)} %fusion.27) | copy-start | bytes 1572868
  655.9 21.7 %copy-start.1 = (bf16[1024,1024]{1,0:T(8,128)(2,1)S(1)}, bf16[1024,1024]{1,0:T(8,128)(2,1)}, u32[]{:S(2)}) copy-start(bf16[1024,1024]{1,0:T(8,128)(2,1)} %param.18) | copy-start | bytes 6291460
Sparse Core Ops, SparseCore 0:
  10.1 85.4 all-gather.5
  168.4 19.5 all-gather.7
  190.8 140.0 all-gather.9
  333.5 139.5 all-gather.11
  475.7 180.2 all-gather.13
  666.5 9.1 reduce-scatter.1
where the time goes:
time: 686 us; the launch traced here: 684 us
  waiting for transfers between devices  531 us (77%)
  matrix products  68.7 us (10%)
  blocking collectives  29.5 us (4%)
  other arithmetic  19.6 us (3%)
  local copies, waits for them, and re-layouts  17.9 us (3%)
  between operations  13.6 us (2%)
    all_gather x1, waiting for transfers between devices, local(): lax.all_gather(down_weight, 'sp', axis=1, tiled=True)  164 us
    all_gather x1, waiting for transfers between devices, local(): lax.all_gather(gate_weight, 'sp', axis=0, tiled=True)  141 us
    all_gather x1, waiting for transfers between devices, local(): lax.all_gather(up_weight, 'sp', axis=0, tiled=True)  134 us
    all_gather x1, waiting for transfers between devices, attend(): arrived = lax.all_gather(keys_values, 'sp', axis=1, tiled=True)  58.6 us
    all_gather x1, blocking collectives, attend(): all_gates = lax.all_gather(cum_gate, 'sp', axis=1, tiled=True)  26.6 us
    dot_general x7, matrix products, add_block(): jnp.einsum('kgtr,krd->kgtd', weights.astype(jnp.bfloat16), values, prefer...  24 us
    all_gather x1, waiting for transfers between devices, local(): lax.all_gather(middle, 'tp', axis=1, tiled=True).astype(jnp.float32)  17.8 us
    dot_general x7, matrix products, add_block(): jnp.einsum('tkgd,krd->kgtr', query_heads, key_part, preferred_element_typ...  17.2 us
  transfers between devices with their start and end apart: 7, of which 7 were waited for; matrix products, arithmetic and copies ran while one was open for 3% of the time, Pallas kernels for 0%

commit v1 on v0

v1 whole, which is shorter than its diff:
```python
import functools

import jax
import jax.numpy as jnp
from jax import lax
from jax.experimental import pallas as pl
from jax.experimental.pallas import tpu as pltpu
from jax.sharding import PartitionSpec as P

norm_eps = 1e-06
log2e = 1.4426950408889634
MESH = pl.DeviceIdType.MESH
VMEM = pl.BlockSpec(memory_space=pltpu.VMEM)
ANY = pl.BlockSpec(memory_space=pl.ANY)


def send_to(src, dst, send_sem, recv_sem, where):
    return pltpu.make_async_remote_copy(
        src_ref=src,
        dst_ref=dst,
        send_sem=send_sem,
        recv_sem=recv_sem,
        device_id=where,
        device_id_type=MESH,
    )


def attend_kernel(
    n, group, wide, q_ref, kv_ref, gate_ref, wgu_ref, wd_ref,
    out_ref, wgu_out, wd_out,
    kv_all, gate_all, max_s, acc_s,
    kv_send, kv_recv, gate_send, gate_recv, gu_send, gu_recv, dn_send, dn_recv, own_sem,
):
    me = lax.axis_index("sp")
    pairs, rows, width = kv_ref.shape
    per_pair = gate_ref.shape[0] // pairs
    dcols = wd_ref.shape[2]

    barrier = pltpu.get_barrier_semaphore()

    def greet(d, c):
        pl.semaphore_signal(barrier, inc=1, device_id={"sp": lax.rem(me + d, n)}, device_id_type=MESH)
        return c

    lax.fori_loop(1, n, greet, 0)
    pl.semaphore_wait(barrier, n - 1)

    def kv_copy(peer, owner):
        return send_to(kv_ref, kv_all.at[owner], kv_send.at[peer], kv_recv.at[owner], {"sp": peer})

    def gate_copy(peer, owner):
        return send_to(gate_ref, gate_all.at[owner], gate_send.at[peer], gate_recv.at[owner], {"sp": peer})

    def wd_slot(owner):
        if wide:
            return wd_out.at[:, pl.ds(pl.multiple_of(owner * dcols, dcols), dcols)]
        return wd_out.at[owner]

    def gu_copy(peer, owner):
        return send_to(
            wgu_ref.at[lax.rem(peer, group)], wgu_out.at[owner], gu_send.at[peer], gu_recv.at[owner], {"sp": peer}
        )

    def dn_copy(peer, owner):
        return send_to(
            wd_ref.at[lax.rem(peer, group)], wd_slot(owner), dn_send.at[peer], dn_recv.at[owner], {"sp": peer}
        )

    def start_kv(d, c):
        gate_copy(me + d, me).start()
        kv_copy(me + d, me).start()
        return c

    lax.fori_loop(1, n - me, start_kv, 0)

    def start_weights(d, c):
        peer = lax.rem(me + d, n)
        gu_copy(peer, me).start()
        dn_copy(peer, me).start()
        return c

    lax.fori_loop(1, n, start_weights, 0)
    own_gu = pltpu.make_async_copy(wgu_ref.at[lax.rem(me, group)], wgu_out.at[me], own_sem.at[0])
    own_dn = pltpu.make_async_copy(wd_ref.at[lax.rem(me, group)], wd_slot(me), own_sem.at[1])
    own_gu.start()
    own_dn.start()

    lanes = lax.broadcasted_iota(jnp.int32, (rows, width), 1)

    def fold(pair, block, gates, first):
        ones_values = jnp.where(lanes < width // 2, jnp.bfloat16(1.0), block)
        for inner in range(per_pair):
            h = pair * per_pair + inner
            scores = lax.dot_general(
                q_ref[h], block, (((1,), (1,)), ((), ())), preferred_element_type=jnp.float32
            )
            scores = scores * log2e - gates[h : h + 1, :] * log2e
            if first:
                r = lax.broadcasted_iota(jnp.int32, scores.shape, 0)
                c = lax.broadcasted_iota(jnp.int32, scores.shape, 1)
                scores = jnp.where(r >= c, scores, -1e30)
            top = jnp.max(scores, axis=1, keepdims=True)
            if first:
                weights = jnp.exp2(scores - top).astype(jnp.bfloat16)
                acc_s[h] = jnp.dot(weights, ones_values, preferred_element_type=jnp.float32)
                max_s[h] = jnp.broadcast_to(top, (scores.shape[0], width))
            else:
                old = max_s[h]
                top = jnp.maximum(old, top)
                weights = jnp.exp2(scores - top[:, :1]).astype(jnp.bfloat16)
                acc_s[h] = acc_s[h] * jnp.exp2(old - top) + jnp.dot(
                    weights, ones_values, preferred_element_type=jnp.float32
                )
                max_s[h] = top

    own_gates = gate_ref[...]
    for pair in range(pairs):
        fold(pair, kv_ref[pair], own_gates, True)

    def earlier(d, c):
        owner = me - d
        gate_copy(me, owner).wait_recv()
        kv_copy(me, owner).wait_recv()
        gates = gate_all[owner]
        for pair in range(pairs):
            fold(pair, kv_all[owner, pair], gates, False)
        return c

    lax.fori_loop(1, me + 1, earlier, 0)
    for h in range(pairs * per_pair):
        acc = acc_s[h]
        out_ref[h] = (acc[:, width // 2 :] / acc[:, : width // 2]).astype(jnp.bfloat16)

    def end_kv(d, c):
        gate_copy(me + d, me).wait_send()
        kv_copy(me + d, me).wait_send()
        return c

    lax.fori_loop(1, n - me, end_kv, 0)

    def end_weights(d, c):
        peer = lax.rem(me + d, n)
        gu_copy(peer, me).wait_send()
        dn_copy(peer, me).wait_send()
        owner = lax.rem(me - d + n, n)
        gu_copy(owner, owner).wait_recv()
        dn_copy(owner, owner).wait_recv()
        return c

    lax.fori_loop(1, n, end_weights, 0)
    own_gu.wait()
    own_dn.wait()


def attend(queries, keys_values, cum_gate, wgu, wd, n, group):
    tok_rows = queries.shape[0]
    pairs, rows, width = keys_values.shape
    heads = cum_gate.shape[0]
    head_dim = width // 2
    q = (queries * (head_dim**-0.5)).astype(jnp.bfloat16).reshape(tok_rows, heads, head_dim)
    q = jnp.pad(q.transpose(1, 0, 2), ((0, 0), (0, 0), (0, head_dim)))
    _, hid, dcols = wd.shape
    wide = dcols % 128 == 0
    dma = pltpu.SemaphoreType.DMA
    out, wgu_all, wd_all = pl.pallas_call(
        functools.partial(attend_kernel, n, group, wide),
        out_shape=(
            jax.ShapeDtypeStruct((heads, tok_rows, head_dim), jnp.bfloat16),
            jax.ShapeDtypeStruct((n,) + wgu.shape[1:], jnp.bfloat16),
            jax.ShapeDtypeStruct((hid, n * dcols) if wide else (n, hid, dcols), jnp.bfloat16),
        ),
        in_specs=[VMEM] * 5,
        out_specs=(VMEM, ANY, ANY),
        scratch_shapes=[
            pltpu.VMEM((n, pairs, rows, width), jnp.bfloat16),
            pltpu.VMEM((n, heads, rows), jnp.float32),
            pltpu.VMEM((heads, tok_rows, width), jnp.float32),
            pltpu.VMEM((heads, tok_rows, width), jnp.float32),
        ]
        + [dma((n,))] * 8
        + [dma((2,))],
        compiler_params=pltpu.CompilerParams(collective_id=0, has_side_effects=True, vmem_limit_bytes=40 << 20),
        cost_estimate=pl.CostEstimate(flops=10**10, bytes_accessed=10**7, transcendentals=10**7),
        name="attend",
    )(q, keys_values, cum_gate, wgu, wd)
    if not wide:
        wd_all = wd_all.transpose(1, 0, 2).reshape(hid, n * dcols)
    attn = out.transpose(1, 0, 2).reshape(tok_rows, heads * head_dim)
    return attn, wgu_all.reshape(-1, wgu.shape[2]), wd_all


def greet_all(group, tp):
    me, mt = lax.axis_index("sp"), lax.axis_index("tp")
    base = me - lax.rem(me, group)
    barrier = pltpu.get_barrier_semaphore()
    for d in range(1, group):
        peer = base + lax.rem(me + d, group)
        pl.semaphore_signal(barrier, inc=1, device_id={"sp": peer, "tp": mt}, device_id_type=MESH)
    for e in range(1, tp):
        other = lax.rem(mt + e, tp)
        pl.semaphore_signal(barrier, inc=1, device_id={"sp": me, "tp": other}, device_id_type=MESH)
    pl.semaphore_wait(barrier, group + tp - 2)
    return me, mt, base


def gather_kernel(group, tp, x_ref, out_ref, own_sem, s1, r1, s2, r2):
    rows, cols = x_ref.shape
    me, mt, base = greet_all(group, tp)
    mine = lax.rem(me, group)

    def slot(b, t):
        return out_ref.at[
            pl.ds(pl.multiple_of(b * rows, rows), rows), pl.ds(pl.multiple_of(t * cols, cols), cols)
        ]

    def across(peer_b, owner_b):
        return send_to(
            x_ref, slot(owner_b, mt), s1.at[peer_b], r1.at[owner_b], {"sp": base + peer_b, "tp": mt}
        )

    def within(src, b, other, owner_t):
        return send_to(src, slot(b, owner_t), s2.at[b, other], r2.at[b, owner_t], {"sp": me, "tp": other})

    own = pltpu.make_async_copy(x_ref, slot(mine, mt), own_sem)
    for d in range(1, group):
        across(lax.rem(mine + d, group), mine).start()
    own.start()
    for e in range(1, tp):
        within(x_ref, mine, lax.rem(mt + e, tp), mt).start()
    for d in range(1, group):
        b = lax.rem(mine - d + group, group)
        across(b, b).wait_recv()
        for e in range(1, tp):
            within(slot(b, mt), b, lax.rem(mt + e, tp), mt).start()
    own.wait()
    for d in range(1, group):
        across(lax.rem(mine + d, group), mine).wait_send()
    for d in range(group):
        b = lax.rem(mine - d + group, group)
        for e in range(1, tp):
            other = lax.rem(mt + e, tp)
            src = x_ref if d == 0 else slot(b, mt)
            within(src, b, other, mt).wait_send()
            within(src, b, other, other).wait_recv()


def gather_tokens(x, group, tp):
    rows, cols = x.shape
    dma = pltpu.SemaphoreType.DMA
    return pl.pallas_call(
        functools.partial(gather_kernel, group, tp),
        out_shape=jax.ShapeDtypeStruct((group * rows, tp * cols), x.dtype),
        in_specs=[VMEM],
        out_specs=VMEM,
        scratch_shapes=[dma, dma((group,)), dma((group,)), dma((group, tp)), dma((group, tp))],
        compiler_params=pltpu.CompilerParams(collective_id=1, has_side_effects=True, vmem_limit_bytes=40 << 20),
        name="gather_tokens",
    )(x)


def scatter_kernel(group, tp, part_ref, out_ref, arrived, summed, s1, r1, s2, r2):
    me, mt, base = greet_all(group, tp)
    mine = lax.rem(me, group)
    rows, cols = out_ref.shape[1:]

    def piece(b, t):
        return part_ref.at[
            pl.ds(pl.multiple_of(b * rows, rows), rows), pl.ds(pl.multiple_of(t * cols, cols), cols)
        ]

    def within(b, other, owner_t):
        return send_to(
            piece(b, other), arrived.at[b, owner_t], s1.at[b, other], r1.at[b, owner_t], {"sp": me, "tp": other}
        )

    def across(peer_b, owner_b):
        return send_to(
            summed.at[peer_b], out_ref.at[owner_b], s2.at[peer_b], r2.at[owner_b], {"sp": base + peer_b, "tp": mt}
        )

    for d in range(1, group + 1):
        b = lax.rem(mine + d, group)
        for e in range(1, tp):
            within(b, lax.rem(mt + e, tp), mt).start()
    for d in range(1, group + 1):
        b = lax.rem(mine + d, group)
        total = piece(b, mt)[...].astype(jnp.float32)
        for e in range(1, tp):
            other = lax.rem(mt + e, tp)
            within(b, other, other).wait_recv()
            total = total + arrived[b, other].astype(jnp.float32)
        if d < group:
            summed[b] = total.astype(jnp.bfloat16)
            across(b, mine).start()
        else:
            out_ref[mine] = total.astype(jnp.bfloat16)
    for d in range(1, group):
        b = lax.rem(mine + d, group)
        across(b, mine).wait_send()
        across(b, b).wait_recv()
    for b in range(group):
        for e in range(1, tp):
            within(b, lax.rem(mt + e, tp), mt).wait_send()


def scatter_sums(partials, group, tp):
    rows, cols = partials.shape[0] // group, partials.shape[1] // tp
    dma = pltpu.SemaphoreType.DMA
    return pl.pallas_call(
        functools.partial(scatter_kernel, group, tp),
        out_shape=jax.ShapeDtypeStruct((group, rows, cols), partials.dtype),
        in_specs=[VMEM],
        out_specs=VMEM,
        scratch_shapes=[
            pltpu.VMEM((group, tp, rows, cols), jnp.bfloat16),
            pltpu.VMEM((group, rows, cols), jnp.bfloat16),
            dma((group, tp)), dma((group, tp)), dma((group,)), dma((group,)),
        ],
        compiler_params=pltpu.CompilerParams(collective_id=2, has_side_effects=True, vmem_limit_bytes=40 << 20),
        name="scatter_sums",
    )(partials)


def local(
    n, tp, group,
    resid, queries, keys_values, cum_gate, out_weight, norm_gain,
    gate_weight, up_weight, conv_kernel, down_weight,
):
    tok_rows = resid.shape[0]
    wrows, hidden_cols = gate_weight.shape
    piece = hidden_cols // group
    wgu = jnp.concatenate(
        [gate_weight.reshape(wrows, group, piece), up_weight.reshape(wrows, group, piece)], axis=2
    ).transpose(1, 0, 2)
    wd = down_weight.reshape(group, piece, down_weight.shape[1])
    attn, wgu_all, wd_all = attend(queries, keys_values, cum_gate, wgu, wd, n, group)
    branch = jnp.dot(
        lax.all_gather(attn, "tp", axis=1, tiled=True),
        out_weight,
        preferred_element_type=jnp.float32,
    )
    middle = (resid.astype(jnp.float32) + branch).astype(jnp.bfloat16)
    middle_full = gather_tokens(middle, group, tp).astype(jnp.float32)
    inverse = lax.rsqrt(jnp.mean(middle_full * middle_full, axis=1, keepdims=True) + norm_eps)
    normed = (middle_full * inverse * norm_gain).astype(jnp.bfloat16)
    joined = jnp.dot(normed, wgu_all, preferred_element_type=jnp.float32).astype(jnp.bfloat16)
    taps = conv_kernel.shape[0]
    reach_back = taps - 1
    all_rows = joined.shape[0]
    pairs = [(i, i + group) for i in range(n) if i + group < n]
    before = lax.ppermute(joined[all_rows - reach_back :], "sp", pairs)
    padded = jnp.concatenate([before, joined], axis=0).astype(jnp.float32)
    at = lax.rem(lax.axis_index("sp"), group) * piece
    kernel = lax.dynamic_slice_in_dim(conv_kernel, at, piece, 2).reshape(taps, 2 * piece)
    mixed = jnp.zeros((all_rows, 2 * piece), jnp.float32)
    for offset in range(taps):
        mixed = mixed + kernel[offset][None, :] * padded[offset : offset + all_rows]
    hidden = (jax.nn.silu(mixed[:, :piece]) * mixed[:, piece:]).astype(jnp.bfloat16)
    partials = jnp.dot(hidden, wd_all, preferred_element_type=jnp.float32).astype(jnp.bfloat16)
    shares = scatter_sums(partials, group, tp).astype(jnp.float32)
    return (middle.astype(jnp.float32) + jnp.sum(shares, axis=0)).astype(jnp.bfloat16)


def solution(mesh):
    n, tp = mesh.shape["sp"], mesh.shape["tp"]
    group = next(g for g in (4, 2, 1) if n % g == 0)
    return jax.shard_map(
        functools.partial(local, n, tp, group),
        mesh=mesh,
        in_specs=(
            P("sp", "tp"),
            P("sp", "tp"),
            P("tp", "sp", None),
            P("tp", "sp"),
            P(None, "tp"),
            P(),
            P("sp", "tp"),
            P("sp", "tp"),
            P(None, None, "tp"),
            P("tp", "sp"),
        ),
        out_specs=P("sp", "tp"),
        check_vma=False,
    )
```

time: 686 us -> 437 us (0.64)
  waiting for transfers between devices: 531 us -> 1.82 us
  Pallas kernels: 0 us -> 391 us
  matrix products: 68.7 us -> 13 us
  blocking collectives: 29.5 us -> 4.47 us
  between operations: 13.6 us -> 0.25 us
  other arithmetic: 19.6 us -> 8.19 us
    all_gather x5 -> x0, waiting for transfers between devices: 516 us -> none  [the longest x1 164 us: local(): lax.all_gather(down_weight, 'sp', axis=1, tiled=True)]
    pallas_call x0 -> x3, Pallas kernels: none -> 391 us  [the longest x1 300 us: attend(): pl.pallas_call(functools.partial(attend_kernel, n, group, wide), out_shap...]
    dot_general x17 -> x2, matrix products: 67.2 us -> 11.1 us  [the longest x1 7.16 us: local(): jnp.dot(normed, wgu_all, preferred_element_type=jnp.float32)]
    all_gather x1 -> x0, blocking collectives: 26.6 us -> none  [attend(): all_gates = lax.all_gather(cum_gate, 'sp', axis=1, tiled=True)]
    cond x21 -> x0, local copies, waits for them, and re-layouts: 13.8 us -> none
    reduce_sum x7 -> x1, other arithmetic: 10.5 us -> 0.39 us  [local(): jnp.sum(shares, axis=0)]
    reduce_scatter x1 -> x0, waiting for transfers between devices: 9.28 us -> none  [local(): lax.psum_scatter(partials.astype(jnp.bfloat16), 'tp', scatter_dimension=1...]
    unnamed x14 -> x25, local copies, waits for them, and re-layouts: 3.77 us -> 10.9 us
  transfers between devices with their start and end apart: 7 -> 1, of which waited for: 7 -> 1; matrix products, arithmetic and copies ran while one was open for 3% -> 0% of each run, Pallas kernels for 0% -> 0%
where the time goes in v1:
time: 437 us
  Pallas kernels  391 us (89%)
  local copies, waits for them, and re-layouts  16.7 us (4%)
  matrix products  13 us (3%)
  other arithmetic  8.19 us (2%)
  blocking collectives  4.47 us (1%)
    pallas_call x1, Pallas kernels, attend(): pl.pallas_call(functools.partial(attend_kernel, n, group, wide), out_shap...  300 us
    pallas_call x1, Pallas kernels, gather_tokens(): pl.pallas_call(functools.partial(gather_kernel, group, tp), out_shape=jax...  62.5 us
    pallas_call x1, Pallas kernels, scatter_sums(): pl.pallas_call(functools.partial(scatter_kernel, group, tp), out_shape=ja...  28.8 us
    unnamed x25, local copies, waits for them, and re-layouts  10.9 us
  transfers between devices with their start and end apart: 1, of which 1 were waited for; matrix products, arithmetic and copies ran while one was open for 0% of the time, Pallas kernels for 0%

profile of v1, /device:TPU:25, one launch (start us, length us, event | category | flops | bytes accessed | tf_op | source)
XLA Modules:
  0.0 436.8 jit_solution(11373742046260277352)
XLA Ops:
  0.0 1.2 copy.11
  1.3 1.0 copy.12
  2.3 1.5 copy.14
  3.8 1.2 copy.16
  4.9 1.5 copy.13
  6.4 1.2 copy.15
  7.6 1.2 pad.4.q_ref
  8.8 1.8 maximum_bitcast_fusion.wgu_ref
  10.6 0.9 copy-done.2
  11.6 299.7 %attend.1 = (bf16[8,256,64]{2,1,0:T(8,128)(2,1)S(1)}, bf16[16,128,1408]{2,1,0:T(8,128)(2,1)S(1)}, bf16[704,2048]{1,0:T(8,128)(2,1)S(1)}) custom-call(bf16[8,256,128]{2,1,0:T(8,128)(2,1)S(1)} %pad.4.q_ref, bf16[4,256,128]{2,1,0:T(8,128)(2,1)S(1)} %copy-done.2, f32[8,256]{1,0:T(8,128)S(1)} %copy-done.3, bf16[4,128,1408]{2,1,0:T(8,128)(2,1)S(1)} %maximum_bitcast_fusion.wgu_ref, ...), custom_call_target="tpu_custom_call" | custom-call | flops 10000000000 | bytes 10000000 | tf_op jit(solution)/shard_map/attend/pallas_call | solution.py:165
  311.2 2.5 copy-done.4
  313.7 1.6 copy-done.5
  315.3 0.2 copy.17
  315.6 4.5 %all_gather.3 = bf16[256,1024]{0,1:T(8,128)(2,1)S(1)} all-gather(bf16[256,512]{0,1:T(8,128)(2,1)S(1)} %bitcast.22), channel_id=1, replica_groups=mesh['sp'=16,'tp'=2] {'tp'}, dimensions={1}, use_global_device_ids=true | all-gather | bytes 786432 | tf_op jit(solution)/shard_map/all_gather | solution.py:338
  320.0 1.9 fusion.15.x_ref
  322.0 62.5 %gather_tokens.1 = bf16[1024,2048]{1,0:T(8,128)(2,1)S(1)} custom-call(bf16[256,1024]{1,0:T(8,128)(2,1)S(1)} %fusion.15.x_ref), custom_call_target="tpu_custom_call" | custom-call | tf_op jit(solution)/shard_map/gather_tokens/pallas_call | solution.py:250
  384.4 0.9 fusion
  385.4 7.2 %fusion.9 = bf16[1024,1408]{1,0:T(8,128)(2,1)S(1)} fusion(bf16[2048,1408]{1,0:T(8,128)(2,1)S(1)} %bitcast.18, bf16[1024,2048]{1,0:T(8,128)(2,1)S(1)} %gather_tokens.1, f32[2048]{0:T(1024)S(1)} %copy-done.8, f32[1024]{0:T(1024)S(1)} %add_rsqrt_fusion), kind=kOutput, calls=%fused_computation.14 | convolution fusion | flops 5915410432 | bytes 12857344 | tf_op jit(solution)/shard_map/dot_general | solution.py:346
  392.6 1.6 copy-done.7
  394.1 1.5 collective-permute-start
  395.6 0.8 constant_dynamic-slice_fusion.1
  396.4 0.1 mul.79
  396.5 0.1 mul.76
  396.6 0.1 mul.68
  396.7 1.8 collective-permute-done
  398.5 2.4 maximum_convert_fusion
  400.9 1.7 fusion.3
  402.6 0.1 copy-done.6
  402.7 3.9 convolution_convert_fusion.part_ref
  406.6 28.8 %scatter_sums.1 = bf16[4,256,1024]{2,1,0:T(8,128)(2,1)S(1)} custom-call(bf16[1024,2048]{1,0:T(8,128)(2,1)S(1)} %convolution_convert_fusion.part_ref), custom_call_target="tpu_custom_call" | custom-call | tf_op jit(solution)/shard_map/scatter_sums/pallas_call | solution.py:309
  435.4 0.4 convert_reduce_fusion
  435.8 1.0 add_convert_fusion
  (21 shorter events, 0.1 us)
Async XLA Ops:
  0.0 320.0 %copy-start = (bf16[1024,1024]{1,0:T(8,128)(2,1)S(1)}, bf16[1024,1024]{1,0:T(8,128)(2,1)}, u32[]{:S(2)}) copy-start(bf16[1024,1024]{1,0:T(8,128)(2,1)} %param.14) | copy-start | bytes 6291460
  3.7 6.9 %copy-start.1 = (bf16[2816,128]{1,0:T(8,128)(2,1)S(1)}, bf16[2816,128]{1,0:T(8,128)(2,1)}, u32[]{:S(2)}) copy-start(bf16[2816,128]{1,0:T(8,128)(2,1)} %param.19) | copy-start | bytes 2162692
  3.7 6.8 %copy-start.3 = (f32[8,256]{1,0:T(8,128)S(1)}, f32[8,256]{1,0:T(8,128)}, u32[]{:S(2)}) copy-start(f32[8,256]{1,0:T(8,128)} %gate_ref.1) | copy-start | bytes 24580
  10.6 1.0 copy-start.2
  311.2 2.5 copy-start.4
  313.7 1.6 copy-start.5
  320.0 65.3 %slice-start = ((s8[5767168]{0:T(1024)(128)(4,1)}), s8[4194304]{0:T(1024)(128)(4,1)S(1)}, s32[]{:S(2)}) async-start(s8[5767168]{0:T(1024)(128)(4,1)} %bitcast.16), calls=%async_computation | async-start | bytes 8388608
  322.0 63.4 %slice-start.1 = ((s8[5767168]{0:T(1024)(128)(4,1)}), s8[1572864]{0:T(1024)(128)(4,1)S(1)}, s32[]{:S(2)}) async-start(s8[5767168]{0:T(1024)(128)(4,1)} %bitcast.16), calls=%async_computation.1 | async-start | bytes 3145728
  322.0 63.4 %copy-start.8 = (f32[2048]{0:T(1024)S(1)}, f32[2048]{0:T(1024)}, u32[]{:S(2)}) copy-start(f32[2048]{0:T(1024)} %param.15) | copy-start | bytes 24580
  392.5 1.6 copy-start.7
  394.1 4.4 %collective-permute-start = (bf16[2,1408]{1,0:T(2,128)(2,1)S(1)}, bf16[2,1408]{1,0:T(2,128)(2,1)S(1)}, u32[]{:S(2)}, u32[]{:S(2)}) collective-permute-start(bf16[2,1408]{1,0:T(2,128)(2,1)S(1)} %slice.39), channel_id=1, source_target_pairs={{0,8},{2,10},{4,12},{6,14},{8,16},{10,18},{12,20},{14,22},{16,24},... | collective-permute-start | bytes 16904 | tf_op jit(solution)/shard_map/ppermute | solution.py:351
  400.9 1.8 copy-start.6

commit v2 on v1

--- a/solution.py
+++ b/solution.py
@@ -32,58 +32,98 @@
     kv_send, kv_recv, gate_send, gate_recv, gu_send, gu_recv, dn_send, dn_recv, own_sem,
 ):
     me = lax.axis_index("sp")
+    plane = n // group
+    mine, place = me // plane, lax.rem(me, plane)
     pairs, rows, width = kv_ref.shape
     per_pair = gate_ref.shape[0] // pairs
     dcols = wd_ref.shape[2]
 
     barrier = pltpu.get_barrier_semaphore()
 
-    def greet(d, c):
-        pl.semaphore_signal(barrier, inc=1, device_id={"sp": lax.rem(me + d, n)}, device_id_type=MESH)
-        return c
-
-    lax.fori_loop(1, n, greet, 0)
-    pl.semaphore_wait(barrier, n - 1)
-
-    def kv_copy(peer, owner):
-        return send_to(kv_ref, kv_all.at[owner], kv_send.at[peer], kv_recv.at[owner], {"sp": peer})
-
-    def gate_copy(peer, owner):
-        return send_to(gate_ref, gate_all.at[owner], gate_send.at[peer], gate_recv.at[owner], {"sp": peer})
+    def greet(peer):
+        pl.semaphore_signal(barrier, inc=1, device_id={"sp": peer}, device_id_type=MESH)
+
+    def greet_line(d, c):
+        greet(lax.rem(mine + d, group) * plane + place)
+        return c
+
+    def greet_plane(e, c):
+        greet(mine * plane + lax.rem(place + e, plane))
+        return c
+
+    lax.fori_loop(1, group, greet_line, 0)
+    lax.fori_loop(1, plane, greet_plane, 0)
+    pl.semaphore_wait(barrier, group + plane - 2)
+
+    def kv_copy(src, owner, peer, at):
+        return send_to(src, kv_all.at[owner], kv_send.at[at], kv_recv.at[owner], {"sp": peer})
+
+    def gate_copy(src, owner, peer, at):
+        return send_to(src, gate_all.at[owner], gate_send.at[at], gate_recv.at[owner], {"sp": peer})
 
     def wd_slot(owner):
         if wide:
             return wd_out.at[:, pl.ds(pl.multiple_of(owner * dcols, dcols), dcols)]
         return wd_out.at[owner]
 
-    def gu_copy(peer, owner):
-        return send_to(
-            wgu_ref.at[lax.rem(peer, group)], wgu_out.at[owner], gu_send.at[peer], gu_recv.at[owner], {"sp": peer}
-        )
-
-    def dn_copy(peer, owner):
-        return send_to(
-            wd_ref.at[lax.rem(peer, group)], wd_slot(owner), dn_send.at[peer], dn_recv.at[owner], {"sp": peer}
-        )
-
-    def start_kv(d, c):
-        gate_copy(me + d, me).start()
-        kv_copy(me + d, me).start()
-        return c
-
-    lax.fori_loop(1, n - me, start_kv, 0)
-
-    def start_weights(d, c):
-        peer = lax.rem(me + d, n)
-        gu_copy(peer, me).start()
-        dn_copy(peer, me).start()
-        return c
-
-    lax.fori_loop(1, n, start_weights, 0)
-    own_gu = pltpu.make_async_copy(wgu_ref.at[lax.rem(me, group)], wgu_out.at[me], own_sem.at[0])
-    own_dn = pltpu.make_async_copy(wd_ref.at[lax.rem(me, group)], wd_slot(me), own_sem.at[1])
+    def gu_copy(src, owner, peer, at):
+        return send_to(src, wgu_out.at[owner], gu_send.at[at], gu_recv.at[owner], {"sp": peer})
+
+    def dn_copy(src, owner, peer, at):
+        return send_to(src, wd_slot(owner), dn_send.at[at], dn_recv.at[owner], {"sp": peer})
+
+    def line_kv(d, c):
+        peer = (mine + d) * plane + place
+        gate_copy(gate_ref, me, peer, peer).start()
+        kv_copy(kv_ref, me, peer, peer).start()
+        return c
+
+    def own_plane_kv(e, c):
+        peer = me + e
+        gate_copy(gate_ref, me, peer, peer).start()
+        kv_copy(kv_ref, me, peer, peer).start()
+        return c
+
+    lax.fori_loop(1, group - mine, line_kv, 0)
+    lax.fori_loop(1, plane - place, own_plane_kv, 0)
+
+    def line_weights(d, c):
+        other = lax.rem(mine + d, group)
+        peer = other * plane + place
+        gu_copy(wgu_ref.at[other], me, peer, peer).start()
+        dn_copy(wd_ref.at[other], me, peer, peer).start()
+        return c
+
+    lax.fori_loop(1, group, line_weights, 0)
+    own_gu = pltpu.make_async_copy(wgu_ref.at[mine], wgu_out.at[me], own_sem.at[0])
+    own_dn = pltpu.make_async_copy(wd_ref.at[mine], wd_slot(me), own_sem.at[1])
     own_gu.start()
     own_dn.start()
+
+    def forward_kv(d, c):
+        owner = (mine - d) * plane + place
+        gate_copy(gate_ref, owner, me, me).wait_recv()
+        kv_copy(kv_ref, owner, me, me).wait_recv()
+
+        def out(e, c):
+            to = lax.rem(place + e, plane)
+            peer, at = mine * plane + to, (mine - d) * plane + to
+            gate_copy(gate_all.at[owner], owner, peer, at).start()
+            kv_copy(kv_all.at[owner], owner, peer, at).start()
+            return c
+
+        lax.fori_loop(1, plane, out, 0)
+        return c
+
+    lax.fori_loop(1, mine + 1, forward_kv, 0)
+
+    def own_weights(e, c):
+        peer = mine * plane + lax.rem(place + e, plane)
+        gu_copy(wgu_ref.at[mine], me, peer, peer).start()
+        dn_copy(wd_ref.at[mine], me, peer, peer).start()
+        return c
+
+    lax.fori_loop(1, plane, own_weights, 0)
 
     lanes = lax.broadcasted_iota(jnp.int32, (rows, width), 1)
 
@@ -117,37 +157,94 @@
     for pair in range(pairs):
         fold(pair, kv_ref[pair], own_gates, True)
 
-    def earlier(d, c):
-        owner = me - d
-        gate_copy(me, owner).wait_recv()
-        kv_copy(me, owner).wait_recv()
+    def fold_owner(owner):
         gates = gate_all[owner]
         for pair in range(pairs):
             fold(pair, kv_all[owner, pair], gates, False)
-        return c
-
-    lax.fori_loop(1, me + 1, earlier, 0)
+
+    def stage(j, c):
+        def from_plane(e, c):
+            owner = (mine - j) * plane + lax.rem(place - e + plane, plane)
+            gate_copy(gate_ref, owner, me, me).wait_recv()
+            kv_copy(kv_ref, owner, me, me).wait_recv()
+            fold_owner(owner)
+            return c
+
+        @pl.when(j > 0)
+        def _():
+            other = lax.rem(mine + j, group)
+            owner = other * plane + place
+            gu_copy(wgu_ref.at[mine], owner, me, me).wait_recv()
+            dn_copy(wd_ref.at[mine], owner, me, me).wait_recv()
+
+            def out(e, c):
+                to = lax.rem(place + e, plane)
+                peer, at = mine * plane + to, other * plane + to
+                gu_copy(wgu_out.at[owner], owner, peer, at).start()
+                dn_copy(wd_slot(owner), owner, peer, at).start()
+                return c
+
+            lax.fori_loop(1, plane, out, 0)
+
+            @pl.when(j <= mine)
+            def _():
+                fold_owner((mine - j) * plane + place)
+
+        count = jnp.where(j == 0, place + 1, jnp.where(j <= mine, plane, 1))
+        lax.fori_loop(1, count, from_plane, 0)
+        return c
+
+    lax.fori_loop(0, group, stage, 0)
     for h in range(pairs * per_pair):
         acc = acc_s[h]
         out_ref[h] = (acc[:, width // 2 :] / acc[:, : width // 2]).astype(jnp.bfloat16)
 
-    def end_kv(d, c):
-        gate_copy(me + d, me).wait_send()
-        kv_copy(me + d, me).wait_send()
-        return c
-
-    lax.fori_loop(1, n - me, end_kv, 0)
-
-    def end_weights(d, c):
-        peer = lax.rem(me + d, n)
-        gu_copy(peer, me).wait_send()
-        dn_copy(peer, me).wait_send()
-        owner = lax.rem(me - d + n, n)
-        gu_copy(owner, owner).wait_recv()
-        dn_copy(owner, owner).wait_recv()
-        return c
-
-    lax.fori_loop(1, n, end_weights, 0)
+    def end_kv(at):
+        gate_copy(gate_ref, me, me, at).wait_send()
+        kv_copy(kv_ref, me, me, at).wait_send()
+
+    def end_line_kv(d, c):
+        end_kv((mine + d) * plane + place)
+        return c
+
+    def end_plane_kv(e, c):
+        end_kv(me + e)
+        return c
+
+    def end_forward_kv(d, c):
+        def out(e, c):
+            end_kv((mine - d) * plane + lax.rem(place + e, plane))
+            return c
+
+        lax.fori_loop(1, plane, out, 0)
+        return c
+
+    lax.fori_loop(1, group - mine, end_line_kv, 0)
+    lax.fori_loop(1, plane - place, end_plane_kv, 0)
+    lax.fori_loop(1, mine + 1, end_forward_kv, 0)
+
+    def end_weights(at):
+        gu_copy(wgu_ref.at[mine], me, me, at).wait_send()
+        dn_copy(wd_ref.at[mine], me, me, at).wait_send()
+
+    def end_line(d, c):
+        end_weights(lax.rem(mine + d, group) * plane + place)
+        return c
+
+    lax.fori_loop(1, group, end_line, 0)
+
+    def end_plane(k, c):
+        def out(e, c):
+            at = k * plane + lax.rem(place + e, plane)
+            end_weights(at)
+            gu_copy(wgu_ref.at[mine], at, me, me).wait_recv()
+            dn_copy(wd_ref.at[mine], at, me, me).wait_recv()
+            return c
+
+        lax.fori_loop(1, plane, out, 0)
+        return c
+
+    lax.fori_loop(0, group, end_plane, 0)
     own_gu.wait()
     own_dn.wait()
 
@@ -189,24 +286,23 @@
     return attn, wgu_all.reshape(-1, wgu.shape[2]), wd_all
 
 
-def greet_all(group, tp):
+def greet_all(plane, group, tp):
     me, mt = lax.axis_index("sp"), lax.axis_index("tp")
-    base = me - lax.rem(me, group)
+    mine, place = me // plane, lax.rem(me, plane)
     barrier = pltpu.get_barrier_semaphore()
     for d in range(1, group):
-        peer = base + lax.rem(me + d, group)
+        peer = lax.rem(mine + d, group) * plane + place
         pl.semaphore_signal(barrier, inc=1, device_id={"sp": peer, "tp": mt}, device_id_type=MESH)
     for e in range(1, tp):
         other = lax.rem(mt + e, tp)
         pl.semaphore_signal(barrier, inc=1, device_id={"sp": me, "tp": other}, device_id_type=MESH)
     pl.semaphore_wait(barrier, group + tp - 2)
-    return me, mt, base
-
-
-def gather_kernel(group, tp, x_ref, out_ref, own_sem, s1, r1, s2, r2):
+    return me, mt, mine, place
+
+
+def gather_kernel(plane, group, tp, x_ref, out_ref, own_sem, s1, r1, s2, r2):
     rows, cols = x_ref.shape
-    me, mt, base = greet_all(group, tp)
-    mine = lax.rem(me, group)
+    me, mt, mine, place = greet_all(plane, group, tp)
 
     def slot(b, t):
         return out_ref.at[
@@ -215,7 +311,7 @@
 
     def across(peer_b, owner_b):
         return send_to(
-            x_ref, slot(owner_b, mt), s1.at[peer_b], r1.at[owner_b], {"sp": base + peer_b, "tp": mt}
+            x_ref, slot(owner_b, mt), s1.at[peer_b], r1.at[owner_b], {"sp": peer_b * plane + place, "tp": mt}
         )
 
     def within(src, b, other, owner_t):
@@ -244,11 +340,11 @@
             within(src, b, other, other).wait_recv()
 
 
-def gather_tokens(x, group, tp):
+def gather_tokens(x, plane, group, tp):
     rows, cols = x.shape
     dma = pltpu.SemaphoreType.DMA
     return pl.pallas_call(
-        functools.partial(gather_kernel, group, tp),
+        functools.partial(gather_kernel, plane, group, tp),
         out_shape=jax.ShapeDtypeStruct((group * rows, tp * cols), x.dtype),
         in_specs=[VMEM],
         out_specs=VMEM,
@@ -258,9 +354,8 @@
     )(x)
 
 
-def scatter_kernel(group, tp, part_ref, out_ref, arrived, summed, s1, r1, s2, r2):
-    me, mt, base = greet_all(group, tp)
-    mine = lax.rem(me, group)
+def scatter_kernel(plane, group, tp, part_ref, out_ref, arrived, summed, s1, r1, s2, r2):
+    me, mt, mine, place = greet_all(plane, group, tp)
     rows, cols = out_ref.shape[1:]
 
     def piece(b, t):
@@ -275,7 +370,7 @@
 
     def across(peer_b, owner_b):
         return send_to(
-            summed.at[peer_b], out_ref.at[owner_b], s2.at[peer_b], r2.at[owner_b], {"sp": base + peer_b, "tp": mt}
+            summed.at[peer_b], out_ref.at[owner_b], s2.at[peer_b], r2.at[owner_b], {"sp": peer_b * plane + place, "tp": mt}
         )
 
     for d in range(1, group + 1):
@@ -303,11 +398,11 @@
             within(b, lax.rem(mt + e, tp), mt).wait_send()
 
 
-def scatter_sums(partials, group, tp):
+def scatter_sums(partials, plane, group, tp):
     rows, cols = partials.shape[0] // group, partials.shape[1] // tp
     dma = pltpu.SemaphoreType.DMA
     return pl.pallas_call(
-        functools.partial(scatter_kernel, group, tp),
+        functools.partial(scatter_kernel, plane, group, tp),
         out_shape=jax.ShapeDtypeStruct((group, rows, cols), partials.dtype),
         in_specs=[VMEM],
         out_specs=VMEM,
@@ -327,6 +422,8 @@
     gate_weight, up_weight, conv_kernel, down_weight,
 ):
     tok_rows = resid.shape[0]
+    plane = n // group
+    place = lax.rem(lax.axis_index("sp"), plane)
     wrows, hidden_cols = gate_weight.shape
     piece = hidden_cols // group
     wgu = jnp.concatenate(
@@ -340,24 +437,27 @@
         preferred_element_type=jnp.float32,
     )
     middle = (resid.astype(jnp.float32) + branch).astype(jnp.bfloat16)
-    middle_full = gather_tokens(middle, group, tp).astype(jnp.float32)
+    middle_full = gather_tokens(middle, plane, group, tp).astype(jnp.float32)
     inverse = lax.rsqrt(jnp.mean(middle_full * middle_full, axis=1, keepdims=True) + norm_eps)
     normed = (middle_full * inverse * norm_gain).astype(jnp.bfloat16)
     joined = jnp.dot(normed, wgu_all, preferred_element_type=jnp.float32).astype(jnp.bfloat16)
     taps = conv_kernel.shape[0]
     reach_back = taps - 1
-    all_rows = joined.shape[0]
-    pairs = [(i, i + group) for i in range(n) if i + group < n]
-    before = lax.ppermute(joined[all_rows - reach_back :], "sp", pairs)
-    padded = jnp.concatenate([before, joined], axis=0).astype(jnp.float32)
-    at = lax.rem(lax.axis_index("sp"), group) * piece
+    blocks = joined.reshape(group, tok_rows, 2 * piece)
+    pairs = [(i, i - i % plane + (i + 1) % plane) for i in range(n)]
+    before = lax.ppermute(blocks[:, tok_rows - reach_back :], "sp", pairs)
+    shifted = jnp.concatenate([jnp.zeros_like(before[:1]), before[:-1]], axis=0)
+    before = jnp.where(place == 0, shifted, before)
+    padded = jnp.concatenate([before, blocks], axis=1).astype(jnp.float32)
+    at = (lax.axis_index("sp") // plane) * piece
     kernel = lax.dynamic_slice_in_dim(conv_kernel, at, piece, 2).reshape(taps, 2 * piece)
-    mixed = jnp.zeros((all_rows, 2 * piece), jnp.float32)
+    mixed = jnp.zeros((group, tok_rows, 2 * piece), jnp.float32)
     for offset in range(taps):
-        mixed = mixed + kernel[offset][None, :] * padded[offset : offset + all_rows]
+        mixed = mixed + kernel[offset][None, None, :] * padded[:, offset : offset + tok_rows]
+    mixed = mixed.reshape(group * tok_rows, 2 * piece)
     hidden = (jax.nn.silu(mixed[:, :piece]) * mixed[:, piece:]).astype(jnp.bfloat16)
     partials = jnp.dot(hidden, wd_all, preferred_element_type=jnp.float32).astype(jnp.bfloat16)
-    shares = scatter_sums(partials, group, tp).astype(jnp.float32)
+    shares = scatter_sums(partials, plane, group, tp).astype(jnp.float32)
     return (middle.astype(jnp.float32) + jnp.sum(shares, axis=0)).astype(jnp.bfloat16)
 
 

time: 437 us -> 294 us (0.67)
  Pallas kernels: 391 us -> 246 us
    pallas_call x1, Pallas kernels: 300 us -> 144 us  [attend(): pl.pallas_call(functools.partial(attend_kernel, n, group, wide), out_shap...]
    pallas_call x2, Pallas kernels: 91.2 us -> 102 us  [the longest x1 51.3 us: gather_tokens(): pl.pallas_call(functools.partial(gather_kernel, plane, group, tp), out_sh...]
    unnamed x25 -> x23, local copies, waits for them, and re-layouts: 10.9 us -> 10.9 us
where the time goes in v2:
time: 294 us; the launch traced here: 293 us
  Pallas kernels  246 us (84%)
  local copies, waits for them, and re-layouts  18 us (6%)
  matrix products  14.1 us (5%)
  other arithmetic  8.22 us (3%)
  blocking collectives  3.57 us (1%)
    pallas_call x1, Pallas kernels, attend(): pl.pallas_call(functools.partial(attend_kernel, n, group, wide), out_shap...  144 us
    pallas_call x1, Pallas kernels, gather_tokens(): pl.pallas_call(functools.partial(gather_kernel, plane, group, tp), out_sh...  51.3 us
    pallas_call x1, Pallas kernels, scatter_sums(): pl.pallas_call(functools.partial(scatter_kernel, plane, group, tp), out_s...  50.7 us
    unnamed x23, local copies, waits for them, and re-layouts  10.9 us
    dot_general x1, matrix products, local(): jnp.dot(normed, wgu_all, preferred_element_type=jnp.float32)  8.24 us
  transfers between devices with their start and end apart: 1, of which 1 were waited for; matrix products, arithmetic and copies ran while one was open for 0% of the time, Pallas kernels for 0%

profile of v2, /device:TPU:25, one launch (start us, length us, event | category | flops | bytes accessed | tf_op | source)
XLA Modules:
  0.0 293.0 jit_solution(2808793052712393388)
XLA Ops:
  0.0 1.2 copy.11
  1.3 0.3 copy.12
  1.6 2.3 copy.14
  3.8 2.3 copy.16
  6.2 2.3 copy.13
  8.4 2.3 copy.15
  10.7 0.1 pad.5.q_ref
  10.8 1.8 maximum_bitcast_fusion.wgu_ref
  12.7 0.9 copy-done.2
  13.6 144.2 %attend.1 = (bf16[8,256,64]{2,1,0:T(8,128)(2,1)S(1)}, bf16[16,128,1408]{2,1,0:T(8,128)(2,1)S(1)}, bf16[704,2048]{1,0:T(8,128)(2,1)S(1)}) custom-call(bf16[8,256,128]{2,1,0:T(8,128)(2,1)S(1)} %pad.5.q_ref, bf16[4,256,128]{2,1,0:T(8,128)(2,1)S(1)} %copy-done.2, f32[8,256]{1,0:T(8,128)S(1)} %copy-done.3, bf16[4,128,1408]{2,1,0:T(8,128)(2,1)S(1)} %maximum_bitcast_fusion.wgu_ref, ...), custom_call_target="tpu_custom_call" | custom-call | flops 10000000000 | bytes 10000000 | tf_op jit(solution)/shard_map/attend/pallas_call | solution.py:262
  157.8 2.5 copy-done.4
  160.3 1.6 copy-done.5
  161.9 0.2 copy.17
  162.1 3.6 %all_gather.3 = bf16[256,1024]{0,1:T(8,128)(2,1)S(1)} all-gather(bf16[256,512]{0,1:T(8,128)(2,1)S(1)} %bitcast.25), channel_id=1, replica_groups=mesh['sp'=16,'tp'=2] {'tp'}, dimensions={1}, use_global_device_ids=true | all-gather | bytes 786432 | tf_op jit(solution)/shard_map/all_gather | solution.py:435
  165.7 1.9 fusion.15.x_ref
  167.6 51.3 %gather_tokens.1 = bf16[1024,2048]{1,0:T(8,128)(2,1)S(1)} custom-call(bf16[256,1024]{1,0:T(8,128)(2,1)S(1)} %fusion.15.x_ref), custom_call_target="tpu_custom_call" | custom-call | tf_op jit(solution)/shard_map/gather_tokens/pallas_call | solution.py:346
  219.0 0.9 fusion
  219.9 8.2 %fusion.9 = bf16[1024,1408]{1,0:T(8,128)(2,1)} fusion(bf16[2048,1408]{1,0:T(8,128)(2,1)S(1)} %bitcast.20, bf16[1024,2048]{1,0:T(8,128)(2,1)S(1)} %gather_tokens.1, f32[2048]{0:T(1024)S(1)} %copy-done.7, f32[1024]{0:T(1024)S(1)} %add_rsqrt_fusion), kind=kOutput, calls=%fused_computation.14 | convolution fusion | flops 5915410432 | bytes 12857344 | tf_op jit(solution)/shard_map/dot_general | solution.py:443
  228.2 0.9 slice.43
  229.1 1.2 collective-permute-start
  230.3 0.8 constant_dynamic-slice_fusion.1
  231.1 0.1 mul.79
  231.2 0.1 mul.76
  231.3 0.1 mul.68
  231.4 1.3 collective-permute-done
  232.8 2.4 maximum_convert_fusion
  235.2 1.7 fusion.3
  236.9 0.1 copy-done.6
  237.0 3.9 %convolution_convert_fusion.part_ref = bf16[1024,2048]{1,0:T(8,128)(2,1)S(1)} fusion(bf16[704,2048]{1,0:T(8,128)(2,1)S(1)} %copy-done.6, f32[1024,1408]{1,0:T(8,128)S(1)} %bitcast.21), kind=kOutput, calls=%fused_computation.15 | convolution fusion | flops 2959212544 | bytes 13369344 | tf_op jit(solution)/shard_map/dot_general | solution.py:459
  240.9 50.7 %scatter_sums.1 = bf16[4,256,1024]{2,1,0:T(8,128)(2,1)S(1)} custom-call(bf16[1024,2048]{1,0:T(8,128)(2,1)S(1)} %convolution_convert_fusion.part_ref), custom_call_target="tpu_custom_call" | custom-call | tf_op jit(solution)/shard_map/scatter_sums/pallas_call | solution.py:404
  291.6 0.4 convert_reduce_fusion
  292.0 0.9 add_convert_fusion
  (21 shorter events, 0.1 us)
Async XLA Ops:
  0.0 165.7 %copy-start = (bf16[1024,1024]{1,0:T(8,128)(2,1)S(1)}, bf16[1024,1024]{1,0:T(8,128)(2,1)}, u32[]{:S(2)}) copy-start(bf16[1024,1024]{1,0:T(8,128)(2,1)} %param.14) | copy-start | bytes 6291460
  3.8 8.8 %copy-start.1 = (bf16[2816,128]{1,0:T(8,128)(2,1)S(1)}, bf16[2816,128]{1,0:T(8,128)(2,1)}, u32[]{:S(2)}) copy-start(bf16[2816,128]{1,0:T(8,128)(2,1)} %param.19) | copy-start | bytes 2162692
  3.8 8.8 %copy-start.3 = (f32[8,256]{1,0:T(8,128)S(1)}, f32[8,256]{1,0:T(8,128)}, u32[]{:S(2)}) copy-start(f32[8,256]{1,0:T(8,128)} %gate_ref.1) | copy-start | bytes 24580
  12.7 1.0 copy-start.2
  157.8 2.5 copy-start.4
  160.3 1.6 copy-start.5
  165.7 54.2 %slice-start = ((s8[5767168]{0:T(1024)(128)(4,1)}), s8[4194304]{0:T(1024)(128)(4,1)S(1)}, s32[]{:S(2)}) async-start(s8[5767168]{0:T(1024)(128)(4,1)} %bitcast.18), calls=%async_computation | async-start | bytes 8388608
  167.6 52.3 %slice-start.1 = ((s8[5767168]{0:T(1024)(128)(4,1)}), s8[1572864]{0:T(1024)(128)(4,1)S(1)}, s32[]{:S(2)}) async-start(s8[5767168]{0:T(1024)(128)(4,1)} %bitcast.18), calls=%async_computation.1 | async-start | bytes 3145728
  167.6 52.3 %copy-start.7 = (f32[2048]{0:T(1024)S(1)}, f32[2048]{0:T(1024)}, u32[]{:S(2)}) copy-start(f32[2048]{0:T(1024)} %param.15) | copy-start | bytes 24580
  229.1 3.6 %collective-permute-start = (bf16[4,2,1408]{2,1,0:T(2,128)(2,1)S(1)}, bf16[4,2,1408]{2,1,0:T(2,128)(2,1)S(1)}, u32[]{:S(2)}, u32[]{:S(2)}) collective-permute-start(bf16[4,2,1408]{2,1,0:T(2,128)(2,1)S(1)} %slice.43), channel_id=1, source_target_pairs={{0,2},{2,4},{4,6},{6,0},{8,10},{10,12},{12,14},{14,8},{16,18},{18,... | collective-permute-start | bytes 67592 | tf_op jit(solution)/shard_map/ppermute | solution.py:448
  235.2 1.8 copy-start.6
